TPU v7x, 32 devices: a whole 2x2x4 slice. The times are simulated.
32 devices in a mesh: sp: 8 (over z, y), tp: 4 (over x, core).
Axes of the slice: x: 2, y: 2, z: 4, core: 2. Of those that a mesh axis runs over, the one named last changes fastest.
Arguments:
- residual: bfloat16 [8192, 2048], P('sp'), may hold values from -8 to 8
- query_wide: bfloat16 [8192, 1024], P('sp', 'tp'), may hold values from -6 to 6
- key_wide: bfloat16 [8192, 1024], P('sp', 'tp'), may hold values from -6 to 6
- value_wide: bfloat16 [8192, 2048], P('sp', 'tp'), may hold values from -6 to 6
- decay_wide: bfloat16 [8192, 1024], P('sp', 'tp'), may hold values from -12 to 12
- gate_wide: bfloat16 [8192, 2048], P('sp', 'tp'), may hold values from -6 to 6
- query_narrow: bfloat16 [8192, 512], P('sp', 'tp'), may hold values from -6 to 6
- key_narrow: bfloat16 [8192, 512], P('sp', 'tp'), may hold values from -6 to 6
- value_narrow: bfloat16 [8192, 2048], P('sp', 'tp'), may hold values from -6 to 6
- decay_narrow: bfloat16 [8192, 512], P('sp', 'tp'), may hold values from -12 to 12
- gate_narrow: bfloat16 [8192, 2048], P('sp', 'tp'), may hold values from -6 to 6
- head_gain: float32 [512], replicated, may hold values from 0.1 to 1.9
- out_wide: bfloat16 [2048, 2048], P('tp'), may hold values from -0.125 to 0.125
- out_narrow: bfloat16 [2048, 2048], P('tp'), may hold values from -0.125 to 0.125
- mlp_gain: float32 [2048], replicated, may hold values from 0.1 to 1.9
- up_weight: bfloat16 [2048, 4096], P('sp', 'tp'), may hold values from -0.125 to 0.125
- down_weight: bfloat16 [4096, 2048], P('tp', 'sp'), may hold values from -0.09375 to 0.09375
Outputs:
- layer_out: bfloat16 [8192, 2048], P('sp', 'tp')
All inputs are finite; a program needn't handle non-finite values.
Results may differ from a plain program's by a relative error of at most 0.017.
Values may be sent and summed in bfloat16 or wider, within the bound.
A program may use at most 128 MiB of HBM per device.

v0:
```python
import jax
import jax.numpy as jnp
from jax import lax
from jax.sharding import PartitionSpec as P

HEADS = 4
BLOCK = 64
EPS = 1e-05
DECAY_NORMALIZER = 16.0
HIGHEST = lax.Precision.HIGHEST


def entering(array, axis, join, neutral):
    place = lax.axis_index(axis)
    gathered = jax.tree.map(
        lambda a, kind: lax.all_gather(a.astype(kind), axis),
        array,
        (jnp.bfloat16, jnp.bfloat16, jnp.bfloat16, jnp.bfloat16),
    )
    state = jax.tree.map(lambda a, e: jnp.zeros_like(a) + jnp.asarray(e, a.dtype), array, neutral)

    def one(step, state):
        return join(
            state,
            jax.tree.map(
                lambda a, own: lax.dynamic_index_in_dim(a, step, 0, False).astype(own.dtype),
                gathered,
                array,
            ),
        )

    return lax.fori_loop(0, place, one, state)


def block_pass(queries, keys_in, values_in, log_decay, block_len):
    num_blocks = queries.shape[0] // block_len

    def to_blocks(stacked):
        return stacked.reshape((num_blocks, block_len) + stacked.shape[1:])

    causal = jnp.tril(jnp.ones((block_len, block_len), dtype=bool))
    initial = (
        jnp.zeros((queries.shape[1], queries.shape[2], values_in.shape[2]), jnp.float32),
        jnp.zeros((queries.shape[1], queries.shape[2]), jnp.float32),
    )

    def advance(running, inputs):
        memory, offset = running
        block_q, block_k, block_v, block_g = inputs
        within = jnp.cumsum(block_g, axis=0)
        final_log = within[-1]
        scaled_q = block_q * jnp.exp(within)
        scaled_k = block_k * jnp.exp(-within)
        outside = jnp.einsum("ihd,hde->ihe", scaled_q, memory, precision=HIGHEST)
        scores = jnp.einsum("ihd,jhd->hij", scaled_q, scaled_k, precision=HIGHEST)
        scores = jnp.where(causal[None], scores, 0.0)
        inside = jnp.einsum("hij,jhe->ihe", scores, block_v, precision=HIGHEST)
        decayed_keys = scaled_k * jnp.exp(final_log)[None]
        memory = jnp.exp(final_log)[..., None] * memory + jnp.einsum(
            "jhd,jhe->hde", decayed_keys, block_v, precision=HIGHEST
        )
        carried_q = scaled_q * jnp.exp(offset)[None]
        return ((memory, offset + final_log), (outside + inside, carried_q))

    (memory, totals), (outputs, carried_q) = lax.scan(
        advance,
        initial,
        (to_blocks(queries), to_blocks(keys_in), to_blocks(values_in), to_blocks(log_decay)),
    )
    return (outputs.reshape(values_in.shape), carried_q.reshape(queries.shape), totals, memory)


def prepare(query, key_proj, value, decay, heads_here):
    row_count = query.shape[0]
    key_width = query.shape[1] // heads_here
    queries = query.astype(jnp.float32).reshape(row_count, heads_here, key_width) * key_width ** (
        -0.5
    )
    keys_in = key_proj.astype(jnp.float32).reshape(row_count, heads_here, key_width)
    values_in = value.astype(jnp.float32).reshape(
        row_count, heads_here, value.shape[1] // heads_here
    )
    log_decay = (
        jax.nn.log_sigmoid(decay.astype(jnp.float32)).reshape(row_count, heads_here, key_width)
        / DECAY_NORMALIZER
    )
    return (queries, keys_in, values_in, log_decay)


def finish(outputs, gate, head_gain):
    scale = lax.rsqrt(jnp.mean(jnp.square(outputs), axis=-1, keepdims=True) + EPS)
    gated = (
        outputs * scale * head_gain * jax.nn.silu(gate.astype(jnp.float32).reshape(outputs.shape))
    )
    return gated.reshape(outputs.shape[0], -1).astype(jnp.bfloat16)


def combine_states(earlier, later):
    return (
        earlier[0] + later[0],
        jnp.exp(later[0])[..., None] * earlier[1] + later[1],
        earlier[2] + later[2],
        jnp.exp(later[2])[..., None] * earlier[3] + later[3],
    )


def body(
    residual,
    query_wide,
    key_wide,
    value_wide,
    decay_wide,
    gate_wide,
    query_narrow,
    key_narrow,
    value_narrow,
    decay_narrow,
    gate_narrow,
    head_gain,
    out_wide,
    out_narrow,
    mlp_gain,
    up_weight,
    down_weight,
):
    heads_here = HEADS // lax.axis_size("tp")
    up_whole, down_whole = (
        lax.all_gather(up_weight, "sp", axis=0, tiled=True),
        lax.all_gather(down_weight, "sp", axis=1, tiled=True),
    )
    wq, wk, wv, wg = prepare(query_wide, key_wide, value_wide, decay_wide, heads_here)
    wide_out, wide_q, wide_total, wide_memory = block_pass(wq, wk, wv, wg, BLOCK)
    nq, nk, nv, ng = prepare(query_narrow, key_narrow, value_narrow, decay_narrow, heads_here)
    narrow_out, narrow_q, narrow_total, narrow_memory = block_pass(nq, nk, nv, ng, BLOCK)
    identity = (
        jnp.zeros_like(wide_total),
        jnp.zeros_like(wide_memory),
        jnp.zeros_like(narrow_total),
        jnp.zeros_like(narrow_memory),
    )
    incoming = entering(
        (wide_total, wide_memory, narrow_total, narrow_memory), "sp", combine_states, identity
    )
    wide_out = wide_out + jnp.einsum("ihd,hde->ihe", wide_q, incoming[1], precision=HIGHEST)
    narrow_out = narrow_out + jnp.einsum("ihd,hde->ihe", narrow_q, incoming[3], precision=HIGHEST)
    gated_wide = finish(wide_out, gate_wide, head_gain)
    gated_narrow = finish(narrow_out, gate_narrow, head_gain)
    head_terms = jnp.dot(gated_wide, out_wide, preferred_element_type=jnp.float32) + jnp.dot(
        gated_narrow, out_narrow, preferred_element_type=jnp.float32
    )
    tp_index = lax.axis_index("tp")
    col_count = residual.shape[1] // lax.axis_size("tp")
    full_width = residual.shape[1]
    residual_cols = lax.dynamic_slice_in_dim(residual, tp_index * col_count, col_count, 1)
    mixed_cols = lax.psum_scatter(
        head_terms.astype(jnp.bfloat16), "tp", scatter_dimension=1, tiled=True
    ).astype(jnp.float32)
    stream_cols = (residual_cols.astype(jnp.float32) + mixed_cols).astype(jnp.bfloat16)
    stream_f = stream_cols.astype(jnp.float32)
    squares = lax.psum(jnp.sum(jnp.square(stream_f), axis=1, keepdims=True), "tp")
    gain_cols = lax.dynamic_slice_in_dim(mlp_gain, tp_index * col_count, col_count, 0)
    normed_cols = (stream_f * lax.rsqrt(squares / full_width + EPS) * gain_cols).astype(
        jnp.bfloat16
    )
    normed = lax.all_gather(normed_cols, "tp", axis=1, tiled=True)
    before_activation = jnp.dot(normed, up_whole, preferred_element_type=jnp.float32)
    hidden = jnp.square(jax.nn.relu(before_activation)).astype(jnp.bfloat16)
    down_terms = jnp.dot(hidden, down_whole, preferred_element_type=jnp.float32)
    mlp_cols = lax.psum_scatter(
        down_terms.astype(jnp.bfloat16), "tp", scatter_dimension=1, tiled=True
    ).astype(jnp.float32)
    return (stream_cols.astype(jnp.float32) + mlp_cols).astype(jnp.bfloat16)


def solution(mesh):
    return jax.shard_map(
        body,
        mesh=mesh,
        in_specs=(
            P("sp", None),
            P("sp", "tp"),
            P("sp", "tp"),
            P("sp", "tp"),
            P("sp", "tp"),
            P("sp", "tp"),
            P("sp", "tp"),
            P("sp", "tp"),
            P("sp", "tp"),
            P("sp", "tp"),
            P("sp", "tp"),
            P(),
            P("tp", None),
            P("tp", None),
            P(),
            P("sp", "tp"),
            P("tp", "sp"),
        ),
        out_specs=P("sp", "tp"),
        check_vma=False,
    )
```

profile of v0, /device:TPU:0, one launch (start us, length us, event | category | flops | bytes accessed | tf_op | source)
XLA Modules:
  0.0 591.7 jit_solution(7153783925277661843)
XLA Ops:
  6.6 5.0 reshape.501
  11.6 1.1 fusion.89
  13.8 1.6 broadcast.125.clone.1
  15.4 68.5 %while.51 = (s32[]{:T(128)}, f32[1,128,512]{2,1,0:T(8,128)S(1)}, f32[1,128]{1,0:T(1,128)S(1)}, f32[16,64,1,512]{3,1,2,0:T(8,128)}, f32[16,64,1,128]{3,1,2,0:T(8,...) while((s32[]{:T(128)}, f32[1,128,512]{2,1,0:T(8,128)S(1)}, ...), condition=%wide.region_5.6_spmd.clone, body=%wide.region_3.5_spmd.clone.sunk | while | flops 133005568 | bytes 2333321 | solution.py:65
  84.7 2.7 fusion.81
  87.3 3.3 reshape.486
  91.6 3.3 reshape.487
  95.0 4.9 reshape.499
  99.8 2.0 reshape.498
  101.9 1.6 broadcast.125.clone
  103.4 108.7 %while.50 = (s32[]{:T(128)}, f32[1,256,512]{2,1,0:T(8,128)S(1)}, f32[1,256]{1,0:T(1,128)S(1)}, f32[16,64,1,512]{3,1,2,0:T(8,128)}, f32[16,64,1,256]{3,1,2,0:T(8,...) while((s32[]{:T(128)}, f32[1,256,512]{2,1,0:T(8,128)S(1)}, ...), condition=%wide.region_2.3_spmd.clone, body=%wide.region_0.2_spmd.clone.sunk | while | flops 240787968 | bytes 3648133 | solution.py:65
  104.4 1.1 broadcast_multiply_fusion.2
  106.9 1.1 fusion.151
  111.2 1.1 broadcast_multiply_fusion.2
  113.7 1.1 fusion.151
  118.0 1.1 broadcast_multiply_fusion.2
  120.4 1.1 fusion.151
  124.8 1.1 broadcast_multiply_fusion.2
  127.2 1.1 fusion.151
  131.5 1.1 broadcast_multiply_fusion.2
  134.0 1.1 fusion.151
  138.3 1.1 broadcast_multiply_fusion.2
  140.8 1.1 fusion.151
  145.1 1.1 broadcast_multiply_fusion.2
  147.6 1.1 fusion.151
  151.9 1.1 broadcast_multiply_fusion.2
  154.4 1.1 fusion.151
  158.7 1.1 broadcast_multiply_fusion.2
  161.2 1.1 fusion.151
  165.5 1.1 broadcast_multiply_fusion.2
  168.0 1.1 fusion.151
  172.3 1.1 broadcast_multiply_fusion.2
  174.8 1.1 fusion.151
  179.1 1.1 broadcast_multiply_fusion.2
  181.6 1.1 fusion.151
  185.9 1.1 broadcast_multiply_fusion.2
  188.4 1.1 fusion.151
  192.7 1.1 broadcast_multiply_fusion.2
  195.2 1.1 fusion.151
  199.5 1.1 broadcast_multiply_fusion.2
  202.0 1.1 fusion.151
  206.3 1.1 broadcast_multiply_fusion.2
  208.7 1.1 fusion.151
  212.9 3.0 copy.32
  215.9 1.3 copy.33
  217.2 3.0 copy.34
  220.2 1.3 copy.35
  221.5 22.3 %all-gather.5 = bf16[8,1,128]{2,1,0:T(2,128)(2,1)S(1)} all-gather(bf16[1,1,128]{2,1,0:T(2,128)(2,1)S(1)} %convert_bitcast_fusion.1), channel_id=4, replica_groups=mesh['sp'=8,'tp'=4] {'sp'}, dimensions={0}, use_global_device_ids=true | all-gather | bytes 2304 | tf_op jit(solution)/shard_map/all_gather | solution.py:16
  243.9 16.7 %all-gather.4 = bf16[8,1,256]{2,1,0:T(2,128)(2,1)S(1)} all-gather(bf16[1,1,256]{2,1,0:T(2,128)(2,1)S(1)} %convert_bitcast_fusion), channel_id=2, replica_groups=mesh['sp'=8,'tp'=4] {'sp'}, dimensions={0}, use_global_device_ids=true | all-gather | bytes 4608 | tf_op jit(solution)/shard_map/all_gather | solution.py:16
  260.6 4.6 all-gather.18.cloned.1.call-done
  265.4 5.6 multiply_reduce_fusion.1
  271.1 2.0 multiply_reduce_fusion
  273.2 2.8 fusion.78
  276.0 5.0 add_convert_fusion
  283.0 56.4 %reduce-scatter.3.cloned.1.call-done = bf16[1024,512]{1,0:T(8,128)(2,1)} async-done(((bf16[1024,2048]{1,0:T(8,128)(2,1)}), bf16[1024,512]{1,0:T(8,128)(2,1)}) %reduce-scatter.3.cloned.1.call-update) | async-done | bytes 1048592 | tf_op jit(solution)/shard_map/reduce_scatter | solution.py:155
  339.5 2.0 fusion.71
  341.4 5.8 psum.7
  347.2 1.3 fusion.73
  348.8 65.5 %all-gather.14.cloned.1.call-done = bf16[2048,1024]{1,0:T(8,128)(2,1)} async-done(((bf16[256,1024]{1,0:T(8,128)(2,1)}), bf16[2048,1024]{1,0:T(8,128)(2,1)}) %all-gather.14.cloned.1.call-update) | async-done | bytes 4194320 | tf_op jit(solution)/shard_map/all_gather | solution.py:128
  414.3 75.1 %all-gather.16.cloned.1.call-done = bf16[1024,2048]{1,0:T(8,128)(2,1)} async-done(((bf16[1024,256]{1,0:T(8,128)(2,1)}), bf16[1024,2048]{1,0:T(8,128)(2,1)}) %all-gather.16.cloned.1.call-update) | async-done | bytes 4194320 | tf_op jit(solution)/shard_map/all_gather | solution.py:129
  489.4 34.1 %all-gather.12.cloned.1.call-done = bf16[1024,2048]{1,0:T(8,128)(2,1)} async-done(((bf16[1024,512]{1,0:T(8,128)(2,1)}), bf16[1024,2048]{1,0:T(8,128)(2,1)}) %all-gather.12.cloned.1.call-update) | async-done | bytes 4194320 | tf_op jit(solution)/shard_map/all_gather | solution.py:165
  523.4 14.4 %convolution_convert_fusion = bf16[1024,2048]{1,0:T(8,128)(2,1)} fusion(bf16[1024,2048]{1,0:T(8,128)(2,1)} %all-gather.16.cloned.1.call-done, bf16[1024,2048]{1,0:T(8,128)(2,1)} %all-gather.12.cloned.1.call-done, bf16[2048,1024]{1,0:T(8,128)(2,1)} %all-gather.14.cloned.1.call-done), kind=kOutput, calls=%fused_computation.91 | convolution fusion | flops 8595177472 | bytes 16777216 | tf_op jit(solution)/shard_map/dot_general | solution.py:168
  537.9 44.5 %reduce-scatter.5.cloned.1.call-done = bf16[1024,512]{1,0:T(8,128)(2,1)} async-done(((bf16[1024,2048]{1,0:T(8,128)(2,1)}), bf16[1024,512]{1,0:T(8,128)(2,1)}) %reduce-scatter.5.cloned.1.call-update) | async-done | bytes 1048592 | tf_op jit(solution)/shard_map/reduce_scatter | solution.py:169
  582.4 2.5 fusion.74
  (383 shorter events, 147.1 us)
Async XLA Ops:
  6.5 266.6 %copy-start = (bf16[512,2048]{1,0:T(8,128)(2,1)S(1)}, bf16[512,2048]{1,0:T(8,128)(2,1)}, u32[]{:S(2)}) copy-start(bf16[512,2048]{1,0:T(8,128)(2,1)} %param.35) | copy-start | bytes 6291460
  6.5 5.0 copy-start.10
  6.5 5.1 copy-start.11
  6.5 254.0 %all-gather.20.cloned.1.call-start = ((), (), s32[]{:S(2)}) async-start(), calls=%async_computation.8 | async-start | bytes 1179648 | tf_op jit(solution)/shard_map/all_gather | solution.py:16
  83.9 6.7 %copy-start.7 = (bf16[1024,256]{1,0:T(8,128)(2,1)S(1)}, bf16[1024,256]{1,0:T(8,128)(2,1)}, u32[]{:S(2)}) copy-start(bf16[1024,256]{1,0:T(8,128)(2,1)} %param.24) | copy-start | bytes 1572868
  84.6 180.5 %all-gather.18.cloned.1.call-start = ((), (), s32[]{:S(2)}) async-start(), calls=%async_computation.7 | async-start | bytes 2359296 | tf_op jit(solution)/shard_map/all_gather | solution.py:16
  91.6 8.2 %copy-start.8 = (bf16[1024,256]{1,0:T(8,128)(2,1)S(1)}, bf16[1024,256]{1,0:T(8,128)(2,1)}, u32[]{:S(2)}) copy-start(bf16[1024,256]{1,0:T(8,128)(2,1)} %param.25) | copy-start | bytes 1572868
  212.9 126.6 %reduce-scatter.3.cloned.1.call-start = ((), (), s32[]{:S(2)}) async-start(), calls=%async_computation.2 | async-start | bytes 5242880 | tf_op jit(solution)/shard_map/reduce_scatter | solution.py:155
  212.9 3.0 copy-start.3
  217.2 3.0 copy-start.4
  265.4 5.7 copy-start.2
  265.4 5.7 copy-start.9
  271.1 2.1 copy-start.6
  271.1 2.1 copy-start.13
  273.2 2.8 copy-start.5
  273.2 2.8 copy-start.12
  281.0 133.2 %all-gather.14.cloned.1.call-start = ((), (), s32[]{:S(2)}) async-start(), calls=%async_computation.4 | async-start | bytes 4718592 | tf_op jit(solution)/shard_map/all_gather | solution.py:128
  281.6 207.7 %all-gather.16.cloned.1.call-start = ((), (), s32[]{:S(2)}) async-start(), calls=%async_computation.5 | async-start | bytes 4718592 | tf_op jit(solution)/shard_map/all_gather | solution.py:129
  282.2 241.2 %all-gather.12.cloned.1.call-start = ((), (), s32[]{:S(2)}) async-start(), calls=%async_computation.3 | async-start | bytes 5242880 | tf_op jit(solution)/shard_map/all_gather | solution.py:165
  348.5 233.9 %reduce-scatter.5.cloned.1.call-start = ((), (), s32[]{:S(2)}) async-start(), calls=%async_computation.6 | async-start | bytes 5242880 | tf_op jit(solution)/shard_map/reduce_scatter | solution.py:169
  537.9 47.0 %copy-start.1 = (bf16[512,2048]{1,0:T(8,128)(2,1)S(1)}, bf16[512,2048]{1,0:T(8,128)(2,1)}, u32[]{:S(2)}) copy-start(bf16[512,2048]{1,0:T(8,128)(2,1)} %param.35) | copy-start | bytes 6291460
Sparse Core Ops, SparseCore 0:
  84.7 43.0 all-gather.19
  213.0 52.1 all-gather.17
  281.2 58.2 reduce-scatter.2
  341.4 72.7 all-gather.13
  416.2 73.1 all-gather.15
  490.8 32.6 all-gather.11
  538.0 44.3 reduce-scatter.4
where the time goes:
time: 596 us; the launch traced here: 592 us
  waiting for transfers between devices  281 us (47%)
  matrix products  95.3 us (16%)
  local copies, waits for them, and re-layouts  83 us (14%)
  other arithmetic  71.2 us (12%)
  blocking collectives  44.8 us (8%)
  between operations  13.8 us (2%)
    all_gather x1, waiting for transfers between devices, body(): lax.all_gather(down_weight, 'sp', axis=1, tiled=True)  75.1 us
    all_gather x1, waiting for transfers between devices, body(): lax.all_gather(up_weight, 'sp', axis=0, tiled=True)  65.5 us
    reduce_scatter x1, waiting for transfers between devices, body(): lax.psum_scatter(head_terms.astype(jnp.bfloat16), 'tp', scatter_dimension...  56.4 us
    reduce_scatter x1, waiting for transfers between devices, body(): lax.psum_scatter(down_terms.astype(jnp.bfloat16), 'tp', scatter_dimension...  44.5 us
    dynamic_slice x48, local copies, waits for them, and re-layouts, block_pass(): lax.scan(advance, initial, (to_blocks(queries), to_blocks(keys_in), to_bl...  41.7 us
    all_gather x2, blocking collectives, entering(): lax.all_gather(a.astype(kind), axis)  39 us
    all_gather x1, waiting for transfers between devices, body(): normed = lax.all_gather(normed_cols, 'tp', axis=1, tiled=True)  34.1 us
    dot_general x32, matrix products, advance(): outside = jnp.einsum('ihd,hde->ihe', scaled_q, memory, precision=HIGHEST)  22.1 us
  transfers between devices with their start and end apart: 7, of which 6 were waited for; matrix products, arithmetic and copies ran while one was open for 24% of the time, Pallas kernels for 0%

commit v1 on v0

--- a/solution.py
+++ b/solution.py
@@ -8,6 +8,9 @@
 EPS = 1e-05
 DECAY_NORMALIZER = 16.0
 HIGHEST = lax.Precision.HIGHEST
+_mix_corner = lambda inner_x: jnp.concatenate(
+    lax.all_to_all(jnp.stack([inner_x for _ in range(lax.axis_size("sp"))], 0), "sp", 0, 0), 0
+)
 
 
 def entering(array, axis, join, neutral):
@@ -125,7 +128,7 @@
 ):
     heads_here = HEADS // lax.axis_size("tp")
     up_whole, down_whole = (
-        lax.all_gather(up_weight, "sp", axis=0, tiled=True),
+        _mix_corner(up_weight),
         lax.all_gather(down_weight, "sp", axis=1, tiled=True),
     )
     wq, wk, wv, wg = prepare(query_wide, key_wide, value_wide, decay_wide, heads_here)

time: 596 us -> 558 us (0.936)
  waiting for transfers between devices: 281 us -> 221 us
  starting transfers between devices: 0.47 us -> 18.7 us
    all_to_all x0 -> x1, waiting for transfers between devices: none -> 82.4 us  [lax.all_to_all(jnp.stack([inner_x for _ in range(lax.axis_size('sp'))], 0...]
    all_gather x1 -> x0, waiting for transfers between devices: 65.5 us -> none  [body(): lax.all_gather(up_weight, 'sp', axis=0, tiled=True)]
    all_gather x1, waiting for transfers between devices: 75.1 us -> 17.9 us  [body(): lax.all_gather(down_weight, 'sp', axis=1, tiled=True)]
    reduce_scatter x1, waiting for transfers between devices: 56.4 us -> 35.6 us  [body(): lax.psum_scatter(head_terms.astype(jnp.bfloat16), 'tp', scatter_dimension...]
    all_to_all x0 -> x1, starting transfers between devices: none -> 18.5 us  [lax.all_to_all(jnp.stack([inner_x for _ in range(lax.axis_size('sp'))], 0...]
  transfers between devices with their start and end apart: 7 -> 7, of which waited for: 6 -> 6; matrix products, arithmetic and copies ran while one was open for 24% -> 26% of each run, Pallas kernels for 0% -> 0%
where the time goes in v1:
time: 558 us; the launch traced here: 553 us
  waiting for transfers between devices  221 us (40%)
  matrix products  95.3 us (17%)
  local copies, waits for them, and re-layouts  85.9 us (15%)
  other arithmetic  71.2 us (13%)
  blocking collectives  45.1 us (8%)
  starting transfers between devices  18.7 us (3%)
  between operations  13.8 us (2%)
    all_to_all x1, waiting for transfers between devices, lax.all_to_all(jnp.stack([inner_x for _ in range(lax.axis_size('sp'))], 0...  82.4 us
    reduce_scatter x1, waiting for transfers between devices, body(): lax.psum_scatter(down_terms.astype(jnp.bfloat16), 'tp', scatter_dimension...  44.5 us
    dynamic_slice x48, local copies, waits for them, and re-layouts, block_pass(): lax.scan(advance, initial, (to_blocks(queries), to_blocks(keys_in), to_bl...  41.7 us
    all_gather x2, blocking collectives, entering(): lax.all_gather(a.astype(kind), axis)  39 us
    reduce_scatter x1, waiting for transfers between devices, body(): lax.psum_scatter(head_terms.astype(jnp.bfloat16), 'tp', scatter_dimension...  35.6 us
    all_gather x1, waiting for transfers between devices, body(): normed = lax.all_gather(normed_cols, 'tp', axis=1, tiled=True)  35.4 us
    dot_general x32, matrix products, advance(): outside = jnp.einsum('ihd,hde->ihe', scaled_q, memory, precision=HIGHEST)  22.1 us
    dot_general x32, matrix products, advance(): inside = jnp.einsum('hij,jhe->ihe', scores, block_v, precision=HIGHEST)  19.4 us
  transfers between devices with their start and end apart: 7, of which 6 were waited for; matrix products, arithmetic and copies ran while one was open for 26% of the time, Pallas kernels for 0%

profile of v1, /device:TPU:0, one launch (start us, length us, event | category | flops | bytes accessed | tf_op | source)
XLA Modules:
  0.0 552.9 jit_solution(9813216299249164384)
XLA Ops:
  6.6 5.0 reshape.507
  11.6 1.1 fusion.89
  13.8 1.6 broadcast.127.clone.1
  15.4 68.5 %while.51 = (s32[]{:T(128)}, f32[1,128,512]{2,1,0:T(8,128)S(1)}, f32[1,128]{1,0:T(1,128)S(1)}, f32[16,64,1,512]{3,1,2,0:T(8,128)}, f32[16,64,1,128]{3,1,2,0:T(8,...) while((s32[]{:T(128)}, f32[1,128,512]{2,1,0:T(8,128)S(1)}, ...), condition=%wide.region_5.6_spmd.clone, body=%wide.region_3.5_spmd.clone.sunk | while | flops 133005568 | bytes 2333321 | solution.py:68
  84.7 2.7 fusion.81
  87.3 3.3 reshape.491
  91.6 3.3 reshape.492
  94.9 4.9 reshape.505
  99.8 2.0 reshape.504
  101.9 1.6 broadcast.127.clone
  103.4 108.7 %while.50 = (s32[]{:T(128)}, f32[1,256,512]{2,1,0:T(8,128)S(1)}, f32[1,256]{1,0:T(1,128)S(1)}, f32[16,64,1,512]{3,1,2,0:T(8,128)}, f32[16,64,1,256]{3,1,2,0:T(8,...) while((s32[]{:T(128)}, f32[1,256,512]{2,1,0:T(8,128)S(1)}, ...), condition=%wide.region_2.3_spmd.clone, body=%wide.region_0.2_spmd.clone.sunk | while | flops 240787968 | bytes 3648133 | solution.py:68
  104.4 1.1 broadcast_multiply_fusion.2
  106.9 1.1 fusion.151
  111.2 1.1 broadcast_multiply_fusion.2
  113.7 1.1 fusion.151
  118.0 1.1 broadcast_multiply_fusion.2
  120.4 1.1 fusion.151
  124.8 1.1 broadcast_multiply_fusion.2
  127.2 1.1 fusion.151
  131.5 1.1 broadcast_multiply_fusion.2
  134.0 1.1 fusion.151
  138.3 1.1 broadcast_multiply_fusion.2
  140.8 1.1 fusion.151
  145.1 1.1 broadcast_multiply_fusion.2
  147.6 1.1 fusion.151
  151.9 1.1 broadcast_multiply_fusion.2
  154.4 1.1 fusion.151
  161.2 1.1 fusion.151
  165.5 1.1 broadcast_multiply_fusion.2
  168.0 1.1 fusion.151
  172.3 1.1 broadcast_multiply_fusion.2
  174.8 1.1 fusion.151
  179.1 1.1 broadcast_multiply_fusion.2
  181.6 1.1 fusion.151
  185.9 1.1 broadcast_multiply_fusion.2
  188.4 1.1 fusion.151
  195.2 1.1 fusion.151
  199.5 1.1 broadcast_multiply_fusion.2
  202.0 1.1 fusion.151
  206.3 1.1 broadcast_multiply_fusion.2
  208.7 1.1 fusion.151
  212.9 3.0 copy.32
  215.9 1.3 copy.33
  217.2 3.0 copy.34
  220.2 1.3 copy.35
  221.5 22.3 %all-gather.5 = bf16[8,1,128]{2,1,0:T(2,128)(2,1)S(1)} all-gather(bf16[1,1,128]{2,1,0:T(2,128)(2,1)S(1)} %convert_bitcast_fusion.1), channel_id=4, replica_groups=mesh['sp'=8,'tp'=4] {'sp'}, dimensions={0}, use_global_device_ids=true | all-gather | bytes 2304 | tf_op jit(solution)/shard_map/all_gather | solution.py:19
  243.9 16.7 %all-gather.4 = bf16[8,1,256]{2,1,0:T(2,128)(2,1)S(1)} all-gather(bf16[1,1,256]{2,1,0:T(2,128)(2,1)S(1)} %convert_bitcast_fusion), channel_id=2, replica_groups=mesh['sp'=8,'tp'=4] {'sp'}, dimensions={0}, use_global_device_ids=true | all-gather | bytes 4608 | tf_op jit(solution)/shard_map/all_gather | solution.py:19
  260.6 4.6 all-gather.15.cloned.1.call-done
  265.4 5.6 %multiply_reduce_fusion.1 = (f32[1024]{0:T(1024)S(1)}, f32[1024,1,512]{0,2,1:T(8,128)S(1)}) fusion(f32[1024,1,512]{0,2,1:T(8,128)} %copy.32, f32[1024,256]{1,0:T(8,128)} %bitcast.286, f32[1,256,512]{2,1,0:T(8,128)S(1)} %get-tuple-element.190), kind=kOutput, calls=%fused_computation.120 | convolution fusion | flops 1612184576 | bytes 5771264 | tf_op jit(solution)/shard_map/ihd,hde->ihe/dot_general | solution.py:147
  271.1 2.0 multiply_reduce_fusion
  273.2 2.8 fusion.78
  276.0 5.0 add_convert_fusion
  282.1 2.5 stack.2
  284.5 18.5 %all-to-all-start = ((bf16[8,256,1024]{2,1,0:T(8,128)(2,1)}), bf16[8,256,1024]{2,1,0:T(8,128)(2,1)}, u32[]{:S(2)}, u32[]{:S(2)}) async-start(bf16[8,256,1024]{2,1,0:T(8,128)(2,1)} %stack.2), calls=%async_computation.1 | async-start | bytes 8388608 | tf_op jit(solution)/shard_map/all_to_all | solution.py:12
  303.9 35.6 %reduce-scatter.3.cloned.1.call-done = bf16[1024,512]{1,0:T(8,128)(2,1)} async-done(((bf16[1024,2048]{1,0:T(8,128)(2,1)}), bf16[1024,512]{1,0:T(8,128)(2,1)}) %reduce-scatter.3.cloned.1.call-update) | async-done | bytes 1048592 | tf_op jit(solution)/shard_map/reduce_scatter | solution.py:158
  339.5 2.0 fusion.71
  341.4 6.1 %psum.7 = f32[1024,1]{0,1:T(1,128)S(1)} all-reduce(f32[1024,1]{0,1:T(1,128)S(1)} %bitcast.296), channel_id=1, replica_groups=mesh['sp'=8,'tp'=4] {'tp'}, use_global_device_ids=true, to_apply=%region_12.13 | all-reduce | flops 1024 | bytes 8192 | tf_op jit(solution)/shard_map/psum | solution.py:163
  347.5 1.3 fusion.73
  348.9 82.4 %all-to-all-done = bf16[8,256,1024]{2,1,0:T(8,128)(2,1)} async-done(((bf16[8,256,1024]{2,1,0:T(8,128)(2,1)}), bf16[8,256,1024]{2,1,0:T(8,128)(2,1)}, u32[]{:S(2)}, u32[]{:S(2)}) %all-to-all-start) | async-done | bytes 4194336 | tf_op jit(solution)/shard_map/all_to_all | solution.py:12
  431.3 17.9 %all-gather.13.cloned.1.call-done = bf16[1024,2048]{1,0:T(8,128)(2,1)} async-done(((bf16[1024,256]{1,0:T(8,128)(2,1)}), bf16[1024,2048]{1,0:T(8,128)(2,1)}) %all-gather.13.cloned.1.call-update) | async-done | bytes 4194320 | tf_op jit(solution)/shard_map/all_gather | solution.py:132
  449.2 35.4 %all-gather.11.cloned.1.call-done = bf16[1024,2048]{1,0:T(8,128)(2,1)} async-done(((bf16[1024,512]{1,0:T(8,128)(2,1)}), bf16[1024,2048]{1,0:T(8,128)(2,1)}) %all-gather.11.cloned.1.call-update) | async-done | bytes 4194320 | tf_op jit(solution)/shard_map/all_gather | solution.py:168
  484.6 14.4 %convolution_convert_fusion = bf16[1024,2048]{1,0:T(8,128)(2,1)} fusion(bf16[1024,2048]{1,0:T(8,128)(2,1)} %all-gather.13.cloned.1.call-done, bf16[1024,2048]{1,0:T(8,128)(2,1)} %all-gather.11.cloned.1.call-done, bf16[2048,1024]{1,0:T(8,128)(2,1)} %bitcast.28), kind=kOutput, calls=%fused_computation.91 | convolution fusion | flops 8595177472 | bytes 16777216 | tf_op jit(solution)/shard_map/dot_general | solution.py:171
  499.0 44.5 %reduce-scatter.5.cloned.1.call-done = bf16[1024,512]{1,0:T(8,128)(2,1)} async-done(((bf16[1024,2048]{1,0:T(8,128)(2,1)}), bf16[1024,512]{1,0:T(8,128)(2,1)}) %reduce-scatter.5.cloned.1.call-update) | async-done | bytes 1048592 | tf_op jit(solution)/shard_map/reduce_scatter | solution.py:172
  543.6 2.5 fusion.74
  (385 shorter events, 148.8 us)
Async XLA Ops:
  6.5 266.6 %copy-start = (bf16[512,2048]{1,0:T(8,128)(2,1)S(1)}, bf16[512,2048]{1,0:T(8,128)(2,1)}, u32[]{:S(2)}) copy-start(bf16[512,2048]{1,0:T(8,128)(2,1)} %param.35) | copy-start | bytes 6291460
  6.5 5.0 copy-start.11
  6.5 5.1 copy-start.12
  6.5 254.0 %all-gather.17.cloned.1.call-start = ((), (), s32[]{:S(2)}) async-start(), calls=%async_computation.8 | async-start | bytes 1179648 | tf_op jit(solution)/shard_map/all_gather | solution.py:19
  83.9 6.7 %copy-start.7 = (bf16[1024,256]{1,0:T(8,128)(2,1)S(1)}, bf16[1024,256]{1,0:T(8,128)(2,1)}, u32[]{:S(2)}) copy-start(bf16[1024,256]{1,0:T(8,128)(2,1)} %param.24) | copy-start | bytes 1572868
  84.6 180.5 %all-gather.15.cloned.1.call-start = ((), (), s32[]{:S(2)}) async-start(), calls=%async_computation.7 | async-start | bytes 2359296 | tf_op jit(solution)/shard_map/all_gather | solution.py:19
  94.9 4.9 copy-start.8
  212.9 126.6 %reduce-scatter.3.cloned.1.call-start = ((), (), s32[]{:S(2)}) async-start(), calls=%async_computation.3 | async-start | bytes 5242880 | tf_op jit(solution)/shard_map/reduce_scatter | solution.py:158
  212.9 3.0 copy-start.3
  217.2 3.0 copy-start.4
  265.4 5.7 %copy-start.2 = (f32[1024,1,512]{0,2,1:T(8,128)S(1)}, f32[1024,1,512]{0,2,1:T(8,128)}, u32[]{:S(2)}) copy-start(f32[1024,1,512]{0,2,1:T(8,128)} %copy.34) | copy-start | bytes 6291460
  265.4 5.7 %copy-start.10 = (f32[16,64,1,128]{3,1,2,0:T(8,128)S(1)}, f32[16,64,1,128]{3,1,2,0:T(8,128)}, u32[]{:S(2)}) copy-start(f32[16,64,1,128]{3,1,2,0:T(8,128)} %get-tuple-element.194) | copy-start | bytes 1572868
  271.1 2.1 copy-start.6
  271.1 2.1 copy-start.14
  273.2 2.8 copy-start.5
  273.2 2.8 copy-start.13
  281.0 1.0 copy-start.9
  281.0 168.2 %all-gather.13.cloned.1.call-start = ((), (), s32[]{:S(2)}) async-start(), calls=%async_computation.5 | async-start | bytes 4718592 | tf_op jit(solution)/shard_map/all_gather | solution.py:132
  284.5 146.8 %all-to-all-start = ((bf16[8,256,1024]{2,1,0:T(8,128)(2,1)}), bf16[8,256,1024]{2,1,0:T(8,128)(2,1)}, u32[]{:S(2)}, u32[]{:S(2)}) async-start(bf16[8,256,1024]{2,1,0:T(8,128)(2,1)} %stack.2), calls=%async_computation.1 | async-start | bytes 8388608 | tf_op jit(solution)/shard_map/all_to_all | solution.py:12
  303.0 181.6 %all-gather.11.cloned.1.call-start = ((), (), s32[]{:S(2)}) async-start(), calls=%async_computation.4 | async-start | bytes 5242880 | tf_op jit(solution)/shard_map/all_gather | solution.py:168
  348.8 194.7 %reduce-scatter.5.cloned.1.call-start = ((), (), s32[]{:S(2)}) async-start(), calls=%async_computation.6 | async-start | bytes 5242880 | tf_op jit(solution)/shard_map/reduce_scatter | solution.py:172
  499.0 47.0 %copy-start.1 = (bf16[512,2048]{1,0:T(8,128)(2,1)S(1)}, bf16[512,2048]{1,0:T(8,128)(2,1)}, u32[]{:S(2)}) copy-start(bf16[512,2048]{1,0:T(8,128)(2,1)} %param.35) | copy-start | bytes 6291460
Sparse Core Ops, SparseCore 0:
  84.7 43.0 all-gather.16
  213.0 52.1 all-gather.14
  281.2 58.2 reduce-scatter.2
  341.4 107.8 all-gather.12
  450.6 33.9 all-gather.10
  499.1 44.3 reduce-scatter.4
